TPU v7x, 32 devices: a whole 2x2x4 slice. The times are simulated.
32 devices in a mesh: sp: 8 (over z, y), tp: 4 (over x, core).
Axes of the slice: x: 2, y: 2, z: 4, core: 2. Of those that a mesh axis runs over, the one named last changes fastest.
Arguments:
- residual_in: bfloat16 [3072, 2048], P(('sp', 'tp')), may hold values from -6 to 6
- queries: bfloat16 [3072, 2048], P('sp', 'tp'), may hold values from -180 to 180
- keys: bfloat16 [3072, 2048], P('sp', 'tp'), may hold values from -9 to 9
- values: bfloat16 [3072, 2048], P('sp', 'tp'), may hold values from -6 to 6
- mix_lambda: float32 [16], P('tp'), may hold values from 0.3 to 0.8
- head_gain: float32 [128], replicated, may hold values from 0.1 to 1.9
- out_weight: bfloat16 [2048, 2048], P('tp'), may hold values from -0.125 to 0.125
- norm_gain: float32 [2048], replicated, may hold values from 0.1 to 1.9
- gate_weight: bfloat16 [2048, 5632], P('sp', 'tp'), may hold values from -0.125 to 0.125
- up_weight: bfloat16 [2048, 5632], P('sp', 'tp'), may hold values from -0.125 to 0.125
- down_weight: bfloat16 [5632, 2048], P('tp', 'sp'), may hold values from -0.078125 to 0.078125
Outputs:
- layer_out: bfloat16 [3072, 2048], P(('sp', 'tp'))
All inputs are finite; a program needn't handle non-finite values.
Results may differ from a plain program's by a relative error of at most 0.014.
Values may be sent and summed in bfloat16 or wider, within the bound.
A program may use at most 128 MiB of HBM per device.

v0:
```python
import functools
import math

import jax
import jax.numpy as jnp
from jax import lax
from jax.experimental import pallas as pl
from jax.experimental.pallas import tpu as pltpu
from jax.sharding import Mesh, PartitionSpec as P

DH = 64
VD = 128
LOG2E = 1.4426950408889634


MESH = pl.DeviceIdType.MESH
AXES = ("za", "yb", "tp")


def remote(src, dst, send, recv, **where):
    return pltpu.make_async_remote_copy(
        src_ref=src, dst_ref=dst, send_sem=send, recv_sem=recv, device_id=where, device_id_type=MESH
    )


def front_kernel(n, lam_ref, gain_ref, qkv, w, o_out, w_out, scr, kk, vx, osend,
                 q_s, q_r, y_s, y_r, w_s, w_r, wy_s, wy_r, o_s, o_r, l_s):
    nz, ny, nt, heads, aligned = n
    z, y, t = (lax.axis_index(name) for name in AXES)
    tok, rows = scr.shape[3], osend.shape[1]
    depth = w.shape[2]

    def place(zz, yy):
        at = zz * ny + yy
        return w_out.at[:, pl.ds(pl.multiple_of(at * depth, depth), depth)] if aligned else w_out.at[at]

    barrier = pltpu.get_barrier_semaphore()
    me = z * nt + t
    for i in range(1, nz * nt):
        p = lax.rem(me + i, nz * nt)
        pl.semaphore_signal(barrier, inc=1, device_id={"za": p // nt, "tp": lax.rem(p, nt)}, device_id_type=MESH)
    for f in range(1, ny):
        pl.semaphore_signal(barrier, inc=1, device_id={"yb": lax.rem(y + f, ny)}, device_id_type=MESH)
    pl.semaphore_wait(barrier, nz * nt - 1 + ny - 1)

    def q_copy(d):
        zp = lax.rem(z + d, nz)
        return remote(qkv.at[zp], scr.at[z, y], q_s.at[d], q_r.at[z], za=zp)

    def kv_own(f):
        return remote(qkv.at[z, pl.ds(1, 2)], scr.at[z, y, pl.ds(1, 2)], y_s.at[0, f], y_r.at[z, y],
                      yb=lax.rem(y + f, ny))

    def kv_copy(d, f):
        zp = lax.rem(z + d, nz)
        part = scr.at[zp, y, pl.ds(1, 2)]
        return remote(part, part, y_s.at[d, f], y_r.at[zp, y], yb=lax.rem(y + f, ny))

    def w_copy(d):
        zp = lax.rem(z + d, nz)
        return remote(w.at[zp], place(z, y), w_s.at[d], w_r.at[z], za=zp)

    def w_own(f):
        return remote(w.at[z], place(z, y), wy_s.at[0, f], wy_r.at[z, y], yb=lax.rem(y + f, ny))

    def w_pass(d, f):
        zp = lax.rem(z + d, nz)
        return remote(place(zp, y), place(zp, y), wy_s.at[d, f], wy_r.at[zp, y], yb=lax.rem(y + f, ny))

    for d in range(nz - 1, 0, -1):
        q_copy(d).start()
    for f in range(1, ny):
        kv_own(f).start()
    local = pltpu.make_async_copy(w.at[z], place(z, y), l_s)
    local.start()
    for d in range(nz - 1, 0, -1):
        w_copy(d).start()
    for f in range(1, ny):
        w_own(f).start()
    scr[z, y] = qkv[z]
    for d in range(1, nz):
        zp = lax.rem(z + d, nz)
        remote(qkv.at[z], scr.at[zp, y], q_s.at[d], q_r.at[zp], za=zp).wait_recv()
        for f in range(1, ny):
            kv_copy(d, f).start()
    for d in range(nz):
        zp = lax.rem(z + d, nz)
        for f in range(1, ny):
            yp = lax.rem(y + f, ny)
            part = scr.at[zp, yp, pl.ds(1, 2)]
            remote(part, part, y_s.at[d, f], y_r.at[zp, yp], yb=yp).wait_recv()
    for zz in range(nz):
        for yy in range(ny):
            span = slice((zz * ny + yy) * tok, (zz * ny + yy + 1) * tok)
            kk[span] = scr[zz, yy, 1]
            for h in range(heads):
                vx[span, 2 * h * VD : (2 * h + 1) * VD] = scr[zz, yy, 2, :, h * VD : (h + 1) * VD]
                vx[span, (2 * h + 1) * VD : (2 * h + 2) * VD] = jnp.ones((tok, VD), jnp.bfloat16)

    scale = LOG2E / math.sqrt(DH)

    def o_copy(p):
        return remote(osend.at[p], o_out.at[me], o_s.at[p], o_r.at[me], za=p // nt, tp=lax.rem(p, nt))

    def block(i, carry):
        zq = i // (nt // 2)
        off = lax.rem(i, nt // 2) * (2 * rows)
        for h in range(heads):
            cols = slice(h * VD, (h + 1) * VD)
            q = scr[zq, y, 0, pl.ds(pl.multiple_of(off, 2 * rows), 2 * rows), cols]
            lane = lax.broadcasted_iota(jnp.int32, q.shape, 1)
            maps = []
            for c in range(2):
                qc = jnp.where((lane >= DH) if c else (lane < DH), q, jnp.zeros_like(q))
                s = lax.dot_general(
                    qc, kk[:, cols], (((1,), (1,)), ((), ())), preferred_element_type=jnp.float32
                )
                top = jnp.max(s, axis=-1, keepdims=True)
                e = jnp.exp2((s - top) * scale).astype(jnp.bfloat16)
                o = jnp.dot(
                    e, vx[:, 2 * h * VD : (2 * h + 2) * VD], preferred_element_type=jnp.float32
                )
                maps.append(o[:, :VD] / o[:, VD:])
            mixed = maps[0] - lam_ref[0:1, cols] * maps[1]
            norm = lax.rsqrt(jnp.mean(mixed * mixed, axis=-1, keepdims=True) + 1e-06)
            done = (mixed * norm * gain_ref[...]).astype(jnp.bfloat16)
            osend[2 * i, :, cols] = done[:rows]
            osend[2 * i + 1, :, cols] = done[rows:]
        for j in range(2):
            p = 2 * i + j

            @pl.when(p != me)
            def _():
                o_copy(p).start()

        @pl.when(i == nz * nt // 2 - 2)
        def _():
            w_take(1)

        return carry

    def w_take(d):
        zp = lax.rem(z + d, nz)
        remote(w.at[z], place(zp, y), w_s.at[d], w_r.at[zp], za=zp).wait_recv()
        for f in range(1, ny):
            w_pass(d, f).start()

    lax.fori_loop(0, nz * nt // 2, block, 0)
    o_out[me] = osend[me]
    local.wait()
    for d in range(2, nz):
        w_take(d)
    for i in range(1, nz * nt):
        p = lax.rem(me + i, nz * nt)
        remote(osend.at[p], o_out.at[p], o_s.at[p], o_r.at[p], za=p // nt, tp=lax.rem(p, nt)).wait_recv()
        o_copy(p).wait_send()
    for d in range(nz):
        zp = lax.rem(z + d, nz)
        for f in range(1, ny):
            yp = lax.rem(y + f, ny)
            remote(place(zp, yp), place(zp, yp), wy_s.at[d, f], wy_r.at[zp, yp], yb=yp).wait_recv()
            if d:
                w_pass(d, f).wait_send()
                kv_copy(d, f).wait_send()
            else:
                w_own(f).wait_send()
                kv_own(f).wait_send()
        if d:
            q_copy(d).wait_send()
            w_copy(d).wait_send()


def front(qkv, weights, lam, gain, rows, sizes):
    nz, ny, nt, heads = sizes
    tok, own = qkv.shape[2:]
    hid, depth = weights.shape[1:]
    aligned = depth % 128 == 0
    w_shape = (hid, nz * ny * depth) if aligned else (nz * ny, hid, depth)
    vmem = pl.BlockSpec(memory_space=pltpu.VMEM)
    dma = pltpu.SemaphoreType.DMA
    out, gathered = pl.pallas_call(
        functools.partial(front_kernel, (nz, ny, nt, heads, aligned)),
        out_shape=(
            jax.ShapeDtypeStruct((nz * nt, rows, own), jnp.bfloat16),
            jax.ShapeDtypeStruct(w_shape, jnp.bfloat16),
        ),
        in_specs=[vmem, vmem, vmem, pl.BlockSpec(memory_space=pl.ANY)],
        out_specs=(vmem, pl.BlockSpec(memory_space=pl.ANY)),
        scratch_shapes=[
            pltpu.VMEM((nz, ny, 3, tok, own), jnp.bfloat16),
            pltpu.VMEM((nz * ny * tok, own), jnp.bfloat16),
            pltpu.VMEM((nz * ny * tok, 2 * own), jnp.bfloat16),
            pltpu.VMEM((nz * nt, rows, own), jnp.bfloat16),
            dma((nz,)), dma((nz,)),
            dma((nz, ny)), dma((nz, ny)),
            dma((nz,)), dma((nz,)),
            dma((nz, ny)), dma((nz, ny)),
            dma((nz * nt,)), dma((nz * nt,)),
            dma,
        ],
        compiler_params=pltpu.CompilerParams(
            collective_id=1, has_side_effects=True, vmem_limit_bytes=60 * 1024 * 1024
        ),
        cost_estimate=pl.CostEstimate(
            flops=100_000_000_000, bytes_accessed=20_000_000, transcendentals=0
        ),
    )(jnp.repeat(lam, VD).reshape(1, own), gain.reshape(1, VD), qkv, weights)
    if not aligned:
        gathered = gathered.transpose(1, 0, 2).reshape(hid, nz * ny * depth)
    return out, gathered


def mixer_kernel(n, normed, after, w, out, got, mine, c_send, c_recv, x_send, x_recv, z_send, z_recv,
                 az_s, az_r, ax_s, ax_r, ac_s, ac_r, rc_s, rc_r, rx_s, rx_r, rz_s, rz_r):
    nz, nx = n
    z, y, t = (lax.axis_index(name) for name in AXES)
    x, c = t // 2, lax.rem(t, 2)
    other = 1 - c
    rows, model = normed.shape
    hid = w.shape[0] // 3

    barrier = pltpu.get_barrier_semaphore()
    for d in range(1, nz):
        pl.semaphore_signal(barrier, inc=1, device_id={"za": lax.rem(z + d, nz)}, device_id_type=MESH)
    for e in range(1, nx):
        pl.semaphore_signal(barrier, inc=1, device_id={"tp": lax.rem(x + e, nx) * 2 + c}, device_id_type=MESH)
    pl.semaphore_signal(barrier, inc=1, device_id={"tp": x * 2 + other}, device_id_type=MESH)
    pl.semaphore_wait(barrier, nz + nx - 1)

    def at(d, e):
        return lax.rem(z + d, nz), lax.rem(x + e, nx)

    def slot(d, e, cc):
        zp, xp = at(d, e)
        return got.at[zp, xp, pl.ds(pl.multiple_of(cc * rows, rows), rows)]

    def ag_z(d):
        return remote(normed, slot(0, 0, c), az_s.at[d], az_r.at[z], za=lax.rem(z + d, nz))

    def ag_x(d, e):
        src = slot(d, 0, c) if d else normed
        return remote(src, slot(d, 0, c), ax_s.at[d, e], ax_r.at[lax.rem(z + d, nz), x],
                      tp=lax.rem(x + e, nx) * 2 + c)

    def ag_c(d, e):
        zp, xp = at(d, e)
        src = slot(d, e, c) if (d or e) else normed
        return remote(src, slot(d, e, c), ac_s.at[d, e], ac_r.at[zp, xp], tp=x * 2 + other)

    def rs_c(d, e):
        return remote(c_send.at[d, e], c_recv.at[d, e], rc_s.at[d, e], rc_r.at[d, e], tp=x * 2 + other)

    def rs_x(d, e):
        return remote(x_send.at[d, e], x_recv.at[d, e], rx_s.at[d, e], rx_r.at[d, e],
                      tp=lax.rem(x + e, nx) * 2 + c)

    def rs_z(d):
        return remote(z_send.at[d], z_recv.at[d], rz_s.at[d], rz_r.at[d], za=lax.rem(z + d, nz))

    for d in range(nz - 1, 0, -1):
        ag_z(d).start()
    for e in range(1, nx):
        ag_x(0, e).start()
    ag_c(0, 0).start()
    got[z, x, pl.ds(pl.multiple_of(c * rows, rows), rows)] = normed[...]

    def after_core(d, e):
        rs_c(d, e).wait_recv()
        both = mine[d, e].astype(jnp.float32) + c_recv[d, e].astype(jnp.float32)
        if e:
            x_send[d, e] = both.astype(jnp.bfloat16)
            rs_x(d, e).start()
        else:
            mine[d, e] = both

    def after_x(d):
        total = mine[d, 0]
        for e in range(1, nx):
            rs_x(d, e).wait_recv()
            total = total + x_recv[d, e].astype(jnp.float32)
        if d:
            z_send[d] = total.astype(jnp.bfloat16)
            rs_z(d).start()
        else:
            mine[0, 0] = total

    steps = [(d, e) for d in range(nz) for e in range(nx)]
    contract = (((1,), (1,)), ((), ()))
    for k, (d, e) in enumerate(steps):
        zp, xp = at(d, e)
        if d and e == 0:
            remote(normed, slot(d, 0, c), az_s.at[d], az_r.at[zp], za=zp).wait_recv()
            for f in range(1, nx):
                ag_x(d, f).start()
            ag_c(d, 0).start()
        if e:
            remote(normed, slot(d, e, c), ax_s.at[d, e], ax_r.at[zp, xp], tp=xp * 2 + c).wait_recv()
            ag_c(d, e).start()
        remote(normed, slot(d, e, other), ac_s.at[d, e], ac_r.at[zp, xp], tp=x * 2 + other).wait_recv()
        block = got[zp, xp]
        gate = lax.dot_general(block, w[0:hid], contract, preferred_element_type=jnp.float32)
        up = lax.dot_general(block, w[hid : 2 * hid], contract, preferred_element_type=jnp.float32)
        hidden = (jax.nn.silu(gate) * up).astype(jnp.bfloat16)
        part = jnp.dot(hidden, w[2 * hid :], preferred_element_type=jnp.float32)
        low, high = part[:rows], part[rows:]
        mine[d, e] = jnp.where(c == 0, low, high)
        c_send[d, e] = jnp.where(c == 0, high, low).astype(jnp.bfloat16)
        rs_c(d, e).start()
        if k:
            after_core(*steps[k - 1])
        if d and e == nx - 1:
            after_x(d - 1)
    after_core(*steps[-1])
    after_x(nz - 1)
    total = mine[0, 0]
    for d in range(1, nz):
        rs_z(d).wait_recv()
        total = total + z_recv[d].astype(jnp.float32)
    out[...] = (after[...] + 0.5 * total).astype(jnp.bfloat16)
    for d, e in steps:
        ag_c(d, e).wait_send()
        rs_c(d, e).wait_send()
        if e:
            ag_x(d, e).wait_send()
            rs_x(d, e).wait_send()
        elif d:
            ag_z(d).wait_send()
            rs_z(d).wait_send()


def mixer_call(normed, after, weights, sizes):
    nz, nx = sizes
    rows, model = normed.shape
    dma = pltpu.SemaphoreType.DMA
    vmem = pl.BlockSpec(memory_space=pltpu.VMEM)
    half = (nz, nx, rows, model)
    return pl.pallas_call(
        functools.partial(mixer_kernel, sizes),
        out_shape=jax.ShapeDtypeStruct((rows, model), jnp.bfloat16),
        in_specs=[vmem] * 3,
        out_specs=vmem,
        scratch_shapes=[
            pltpu.VMEM((nz, nx, 2 * rows, model), jnp.bfloat16),
            pltpu.VMEM(half, jnp.float32),
            pltpu.VMEM(half, jnp.bfloat16),
            pltpu.VMEM(half, jnp.bfloat16),
            pltpu.VMEM(half, jnp.bfloat16),
            pltpu.VMEM(half, jnp.bfloat16),
            pltpu.VMEM((nz, rows, model), jnp.bfloat16),
            pltpu.VMEM((nz, rows, model), jnp.bfloat16),
            dma((nz,)), dma((nz,)),
            dma((nz, nx)), dma((nz, nx)),
            dma((nz, nx)), dma((nz, nx)),
            dma((nz, nx)), dma((nz, nx)),
            dma((nz, nx)), dma((nz, nx)),
            dma((nz,)), dma((nz,)),
        ],
        compiler_params=pltpu.CompilerParams(
            collective_id=2, has_side_effects=True, vmem_limit_bytes=62 * 1024 * 1024
        ),
        cost_estimate=pl.CostEstimate(
            flops=100_000_000_000, bytes_accessed=20_000_000, transcendentals=0
        ),
    )(normed, after, weights)


def body(
    residual_in,
    queries,
    keys,
    values,
    mix_lambda,
    head_gain,
    out_weight,
    norm_gain,
    gate_weight,
    up_weight,
    down_weight,
):
    za, yb, tp = (lax.axis_size(name) for name in AXES)
    tok_local, width = queries.shape
    rows, model = residual_in.shape
    heads = mix_lambda.shape[0] // za
    own = width // za

    out_full = lax.all_gather(out_weight, "tp", axis=0, tiled=True)
    qkv = jnp.stack(
        [a.reshape(tok_local, za, own).transpose(1, 0, 2) for a in (queries, keys, values)], 1
    )
    hid = down_weight.shape[0] // za
    weights = jnp.stack(
        [a.reshape(za, hid, -1) for a in (gate_weight.T, up_weight.T, down_weight)], 1
    ).reshape(za, 3 * hid, -1)
    lam = lax.dynamic_slice_in_dim(mix_lambda, lax.axis_index("za") * heads, heads, 0)
    out, weights = front(qkv, weights, lam, head_gain, rows, (za, yb, tp, heads))
    attended = (
        out.reshape(za, tp, rows, own).transpose(2, 1, 0, 3).reshape(rows, tp * width)
    )
    after = residual_in.astype(jnp.float32) + jnp.dot(
        attended, out_full, preferred_element_type=jnp.float32
    )
    row_scale = lax.rsqrt(jnp.mean(after * after, axis=-1, keepdims=True) + 1e-06)
    normed = (after * row_scale * norm_gain).astype(jnp.bfloat16)
    return mixer_call(normed, after, weights, (za, tp // 2))


def solution(mesh):
    sp, tp = mesh.shape["sp"], mesh.shape["tp"]

    def run(*args):
        heads_local = args[4].shape[0] // tp
        za = math.gcd(heads_local, sp)
        cut = Mesh(mesh.devices.reshape(za, sp // za, tp), ("za", "yb", "tp"))
        s = ("za", "yb")
        return jax.shard_map(
            body,
            mesh=cut,
            in_specs=(
                P(("za", "yb", "tp"), None),
                P(s, "tp"),
                P(s, "tp"),
                P(s, "tp"),
                P("tp"),
                P(),
                P("tp", None),
                P(),
                P(s, "tp"),
                P(s, "tp"),
                P("tp", s),
            ),
            out_specs=P(("za", "yb", "tp"), None),
            check_vma=False,
        )(*args)

    return run
```

profile of v0, /device:TPU:0, one launch (start us, length us, event | category | flops | bytes accessed | tf_op | source)
XLA Modules:
  0.0 248.6 jit_solution(6798194314461844565)
XLA Ops:
  6.5 0.0 copy-start.1
  6.5 0.0 copy-start.2
  6.5 0.0 copy-start.3
  6.5 0.0 all-gather.2.cloned.1.call-start
  6.5 0.7 all-gather.2.cloned.1.call-update
  7.3 0.4 copy-done.1
  7.6 0.3 copy.21
  7.9 0.0 copy-done.2
  7.9 0.3 copy.22
  8.2 0.0 copy-done.3
  8.2 0.2 pad_maximum_fusion
  8.5 0.0 copy-start.4
  8.5 0.0 copy-start.5
  8.5 1.5 copy.23
  10.0 0.0 copy-done.4
  10.0 0.0 copy-start.6
  10.0 0.2 copy.19
  10.2 0.0 copy-start.9
  10.2 0.2 copy.20
  10.5 0.0 copy-done.5
  10.5 0.2 copy.15
  10.7 0.2 copy.16
  10.9 0.1 copy-done.6
  11.0 0.2 copy.17
  11.2 0.2 copy.18
  11.4 0.0 copy-done.9
  11.5 0.6 dynamic_slice.5
  12.0 1.2 pad_maximum_fusion.1.qkv
  13.2 1.2 broadcast_in_dim.2.lam_ref
  14.4 0.0 copy-start.7
  14.4 111.7 %shard_map.109 = (bf16[16,96,128]{2,1,0:T(8,128)(2,1)}, bf16[1056,2048]{1,0:T(8,128)(2,1)}) custom-call(f32[1,128]{1,0:T(1,128)} %broadcast_in_dim.2.lam_ref, f32[1,128]{1,0:T(1,128)} %bitcast.40, bf16[4,3,384,128]{3,2,1,0:T(8,128)(2,1)} %pad_maximum_fusion.1.qkv, bf16[4,1056,256]{2,1,0:T(8,128)(2,1)} %bitcast.30), custom_call_target="tpu_custom_call" | custom-call | flops 99999997952 | bytes 20000000 | tf_op jit(solution)/shard_map/pallas_call | solution.py:181
  126.2 1.3 copy.26
  127.5 0.3 reshape.37
  127.8 0.0 copy-start.8
  127.8 0.0 all-gather.2.cloned.1.call-done
  127.8 0.0 copy-done.7
  127.8 5.0 %multiply_reduce_fusion = (f32[96]{0:T(128)S(1)}, f32[96,2048]{1,0:T(8,128)S(1)}) fusion(bf16[96,2048]{1,0:T(8,128)(2,1)S(1)} %reshape.37, bf16[2048,2048]{1,0:T(8,128)(2,1)} %all-gather.2.cloned.1.call-done, bf16[96,2048]{1,0:T(8,128)(2,1)S(1)} %copy-done.7), kind=kOutput, calls=%fused_computation.4 | convolution fusion | flops 806092672 | bytes 9961856 | tf_op jit(solution)/shard_map/dot_general | solution.py:399
  132.8 0.0 copy-start
  132.8 0.0 copy-done.8
  132.8 1.0 multiply_convert_fusion.normed
  133.8 0.0 copy-done
  133.8 106.2 %shard_map.110 = bf16[96,2048]{1,0:T(8,128)(2,1)} custom-call(bf16[96,2048]{1,0:T(8,128)(2,1)} %multiply_convert_fusion.normed, f32[96,2048]{1,0:T(8,128)} %copy-done, bf16[1056,2048]{1,0:T(8,128)(2,1)} %get-tuple-element.8.w), custom_call_target="tpu_custom_call" | custom-call | flops 99999997952 | bytes 20000000 | tf_op jit(solution)/shard_map/pallas_call | solution.py:337
  240.0 1.8 copy.28
  (1 shorter events, 0.0 us)
Async XLA Ops:
  6.5 1.1 copy-start.1
  6.5 1.4 copy-start.2
  6.5 1.7 copy-start.3
  6.5 121.3 %all-gather.2.cloned.1.call-start = ((), (), s32[]{:S(2)}) async-start(), calls=%async_computation | async-start | bytes 10485760 | tf_op jit(solution)/shard_map/all_gather | solution.py:386
  8.5 1.5 copy-start.4
  8.5 2.0 copy-start.5
  10.0 1.0 copy-start.6
  10.2 1.2 copy-start.9
  14.4 113.4 %copy-start.7 = (bf16[96,2048]{1,0:T(8,128)(2,1)S(1)}, bf16[96,2048]{1,0:T(8,128)(2,1)}, u32[]{:S(2)}) copy-start(bf16[96,2048]{1,0:T(8,128)(2,1)} %param.11) | copy-start | bytes 1179652
  127.8 5.1 %copy-start.8 = (f32[2048]{0:T(1024)S(1)}, f32[2048]{0:T(1024)}, u32[]{:S(2)}) copy-start(f32[2048]{0:T(1024)} %param.18) | copy-start | bytes 24580
  132.8 1.0 copy-start
Sparse Core Ops, SparseCore 0:
  8.9 63.0 all-gather.1
where the time goes:
time: 249 us
  Pallas kernels  218 us (88%)
  between operations  13.6 us (5%)
  local copies, waits for them, and re-layouts  9.03 us (4%)
  matrix products  4.98 us (2%)
    pallas_call x1, Pallas kernels, front(): pl.pallas_call(functools.partial(front_kernel, (nz, ny, nt, heads, aligne...  112 us
    pallas_call x1, Pallas kernels, mixer_call(): pl.pallas_call(functools.partial(mixer_kernel, sizes), out_shape=jax.Shap...  106 us
  transfers between devices with their start and end apart: 1, of which 0 were waited for; matrix products, arithmetic and copies ran while one was open for 3% of the time, Pallas kernels for 45%

commit v1 on v0

v1 whole, which is shorter than its diff:
```python
import functools
import math

import jax
import jax.numpy as jnp
from jax import lax
from jax.experimental import pallas as pl
from jax.experimental.pallas import tpu as pltpu
from jax.sharding import Mesh, PartitionSpec as P

DH = 64
VD = 128
LOG2E = 1.4426950408889634

MESH = pl.DeviceIdType.MESH
AXES = ("za", "yb", "xb", "cb")


def remote(src, dst, send, recv, **where):
    return pltpu.make_async_remote_copy(
        src_ref=src, dst_ref=dst, send_sem=send, recv_sem=recv, device_id=where, device_id_type=MESH
    )


def near_first(z, k, nz):
    m = jnp.minimum(z, nz - 1 - z)
    near = z + ((k + 1) // 2 if k % 2 else -(k // 2))
    far = jnp.where(z < nz - 1 - z, k, nz - 1 - k)
    return jnp.where(k <= 2 * m, near, far)


def layer_kernel(n, lam_ref, gain_ref, ngain_ref, res_hbm, q_hbm, k_hbm, v_hbm, ow_hbm, gate_hbm, up_hbm, down_hbm,
                 out, wp,
                 qs, kk, vx, osend, att, ow, res, w, stage, om, oc_send, oc_recv, ox_send, ox_recv,
                 got, mine, c_send, c_recv, z_send, z_recv,
                 in_s, st_s, qz_s, qz_r, ky_s, ky_r, wl_s, wz_s, wz_r, wx_s, wx_r, wy_s, wy_r,
                 wxy_s, wxy_r, wyx_s, wyx_r, o_s, o_r, oc_s, oc_r, ox_s, ox_r,
                 az_s, az_r, ac_s, ac_r, rc_s, rc_r, rz_s, rz_r):
    nz, ny, nx, nc, heads, aligned = n
    z, y, x, c = (lax.axis_index(name) for name in AXES)
    other = nc - 1 - c
    tok, own = qs.shape[1:]
    rows, model = res.shape
    pair = nc * rows
    hid, depth = gate_hbm.shape[0] // nz, gate_hbm.shape[1]
    cut = hid // 16 * 8

    barrier = pltpu.get_barrier_semaphore()
    for d in range(1, nz):
        pl.semaphore_signal(barrier, inc=1, device_id={"za": lax.rem(z + d, nz)}, device_id_type=MESH)
    for f in range(1, ny):
        pl.semaphore_signal(barrier, inc=1, device_id={"yb": lax.rem(y + f, ny)}, device_id_type=MESH)
    for e in range(1, nx):
        pl.semaphore_signal(barrier, inc=1, device_id={"xb": lax.rem(x + e, nx)}, device_id_type=MESH)
    for e in range(1, nc):
        pl.semaphore_signal(barrier, inc=1, device_id={"cb": other}, device_id_type=MESH)
    pl.semaphore_wait(barrier, nz + ny + nx + nc - 4)

    def tokens(zz, yy):
        return pl.ds(pl.multiple_of((zz * ny + yy) * tok, tok), tok)

    def kv_parts(zz, yy):
        at = tokens(zz, yy)
        return [kk.at[at]] + [vx.at[at, 2 * h * VD : (2 * h + 1) * VD] for h in range(heads)]

    def kv_sources(zp):
        base = zp * own
        return [k_hbm.at[:, pl.ds(pl.multiple_of(base, 128), own)]] + [
            v_hbm.at[:, pl.ds(pl.multiple_of(base + h * VD, 128), VD)] for h in range(heads)
        ]

    def q_source(zp):
        return q_hbm.at[:, pl.ds(pl.multiple_of(zp * own, 128), own)]

    nkv = 1 + heads

    def qkv_copies(d):
        zp = lax.rem(z + d, nz)
        pairs = list(zip(kv_sources(zp), kv_parts(z, y))) + [(q_source(zp), qs.at[z])]
        return [remote(s, t, qz_s.at[i, d], qz_r.at[i, z], za=zp) for i, (s, t) in enumerate(pairs)]

    def qkv_take(zp):
        pairs = list(zip(kv_sources(z), kv_parts(zp, y))) + [(q_source(z), qs.at[zp])]
        return [remote(s, t, qz_s.at[i, 0], qz_r.at[i, zp], za=zp) for i, (s, t) in enumerate(pairs)]

    def kv_pass(d, f):
        zp, yp = lax.rem(z + d, nz), lax.rem(y + f, ny)
        to = kv_parts(zp, y)
        fro = to if d else kv_sources(z)
        return [remote(s, t, ky_s.at[i, d, f], ky_r.at[i, zp, y], yb=yp) for i, (s, t) in enumerate(zip(fro, to))]

    def kv_take(zp, yp):
        to = kv_parts(zp, yp)
        return [remote(t, t, ky_s.at[i, 0, 0], ky_r.at[i, zp, yp], yb=yp) for i, t in enumerate(to)]

    mats = (gate_hbm, up_hbm, down_hbm)

    def place(m, xx, zz, yy, start=0, size=hid):
        at = zz * ny + yy
        r = pl.ds(pl.multiple_of(xx * hid + start, 8), size)
        if aligned:
            return w.at[m, r, pl.ds(pl.multiple_of(at * depth, depth), depth)]
        return wp.at[at, m, r]

    every = slice(None)

    def w_copies(d):
        zp = lax.rem(z + d, nz)
        return [
            remote(a.at[pl.ds(pl.multiple_of(zp * hid, 8), hid)], place(m, x, z, y), wz_s.at[m, d], wz_r.at[m, z], za=zp)
            for m, a in enumerate(mats)
        ]

    def w_local():
        return [
            pltpu.make_async_copy(a.at[pl.ds(pl.multiple_of(z * hid, 8), hid)], place(m, x, z, y), wl_s.at[m])
            for m, a in enumerate(mats)
        ]

    def w_x(d, e):
        zp, xp = lax.rem(z + d, nz), lax.rem(x + e, nx)
        at = place(every, x, zp, y)
        return remote(at, at, wx_s.at[d, e], wx_r.at[zp, x], xb=xp)

    def w_y(d, f):
        zp, yp = lax.rem(z + d, nz), lax.rem(y + f, ny)
        at = place(every, x, zp, y)
        return remote(at, at, wy_s.at[d, f], wy_r.at[zp, y], yb=yp)

    def w_xy(d, e, f):
        zp, xp, yp = lax.rem(z + d, nz), lax.rem(x + e, nx), lax.rem(y + f, ny)
        at = place(every, xp, zp, y, 0, cut)
        return remote(at, at, wxy_s.at[d, e, f], wxy_r.at[zp, xp, y], yb=yp)

    def w_yx(d, f, e):
        zp, xp, yp = lax.rem(z + d, nz), lax.rem(x + e, nx), lax.rem(y + f, ny)
        at = place(every, x, zp, yp, cut, hid - cut)
        return remote(at, at, wyx_s.at[d, f, e], wyx_r.at[zp, yp, x], xb=xp)

    def w_spread(d):
        for e in range(1, nx):
            w_x(d, e).start()
        for f in range(1, ny):
            w_y(d, f).start()

    def w_take(d):
        zp = lax.rem(z + d, nz)
        for m, a in enumerate(mats):
            remote(a.at[pl.ds(0, hid)], place(m, x, zp, y), wz_s.at[m, 0], wz_r.at[m, zp], za=zp).wait_recv()
        w_spread(d)

    def w_turn(d):
        zp = lax.rem(z + d, nz)
        for e in range(1, nx):
            xp = lax.rem(x + e, nx)
            at = place(every, xp, zp, y)
            remote(at, at, wx_s.at[d, e], wx_r.at[zp, xp], xb=xp).wait_recv()
            for f in range(1, ny):
                w_xy(d, e, f).start()
        for f in range(1, ny):
            yp = lax.rem(y + f, ny)
            at = place(every, x, zp, yp)
            remote(at, at, wy_s.at[d, f], wy_r.at[zp, yp], yb=yp).wait_recv()
            for e in range(1, nx):
                w_yx(d, f, e).start()

    def w_done():
        for d in range(nz):
            zp = lax.rem(z + d, nz)
            for e in range(1, nx):
                xp = lax.rem(x + e, nx)
                for f in range(1, ny):
                    yp = lax.rem(y + f, ny)
                    at = place(every, xp, zp, yp, 0, cut)
                    remote(at, at, wxy_s.at[d, e, f], wxy_r.at[zp, xp, yp], yb=yp).wait_recv()
                    at = place(every, xp, zp, yp, cut, hid - cut)
                    remote(at, at, wyx_s.at[d, f, e], wyx_r.at[zp, yp, xp], xb=xp).wait_recv()
        if not aligned:
            for at in range(nz * ny):
                copy = pltpu.make_async_copy(wp.at[at], stage, st_s)
                copy.start()
                copy.wait()
                for m in range(3):
                    w[m, :, at * depth : (at + 1) * depth] = stage[m]

    for d in range(nz - 1, 0, -1):
        for copy in qkv_copies(d):
            copy.start()
    for f in range(1, ny):
        for copy in kv_pass(0, f):
            copy.start()
    locals_in = [
        pltpu.make_async_copy(s, t, in_s.at[i])
        for i, (s, t) in enumerate(
            list(zip(kv_sources(z), kv_parts(z, y))) + [(q_source(z), qs.at[z]), (ow_hbm, ow), (res_hbm, res)]
        )
    ]
    for copy in locals_in:
        copy.start()
    for copy in w_local():
        copy.start()
    for d in range(nz - 1, 1, -1):
        for copy in w_copies(d):
            copy.start()
    for h in range(heads):
        vx[:, (2 * h + 1) * VD : (2 * h + 2) * VD] = jnp.ones((vx.shape[0], VD), jnp.bfloat16)
    for copy in w_local():
        copy.wait()
    w_spread(0)
    for copy in locals_in:
        copy.wait()
    for d in range(1, nz):
        zp = lax.rem(z + d, nz)
        for copy in qkv_take(zp):
            copy.wait_recv()
        for f in range(1, ny):
            for copy in kv_pass(d, f):
                copy.start()
    for d in range(nz):
        zp = lax.rem(z + d, nz)
        for f in range(1, ny):
            for copy in kv_take(zp, lax.rem(y + f, ny)):
                copy.wait_recv()
    w_turn(0)

    scale = LOG2E / math.sqrt(DH)
    block_rows = osend.shape[1]
    per = tok // block_rows

    def o_copy(i):
        zq = lax.rem(z + 1 + i // per, nz)
        off = pl.multiple_of(lax.rem(i, per) * block_rows, block_rows)
        to = att.at[pl.ds(off, block_rows), pl.ds(pl.multiple_of(z * own, 128), own)]
        return remote(osend.at[i], to, o_s.at[i], o_r.at[z, lax.rem(i, per)], za=zq)

    def block(i, carry):
        zq = lax.rem(z + 1 + i // per, nz)
        off = pl.multiple_of(lax.rem(i, per) * block_rows, block_rows)
        for h in range(heads):
            cols = slice(h * VD, (h + 1) * VD)
            q = qs[zq, pl.ds(off, block_rows), cols]
            lane = lax.broadcasted_iota(jnp.int32, q.shape, 1)
            maps = []
            for half in range(2):
                qc = jnp.where((lane >= DH) if half else (lane < DH), q, jnp.zeros_like(q))
                s = lax.dot_general(
                    qc, kk[:, cols], (((1,), (1,)), ((), ())), preferred_element_type=jnp.float32
                )
                top = jnp.max(s, axis=-1, keepdims=True)
                e = jnp.exp2((s - top) * scale).astype(jnp.bfloat16)
                o = jnp.dot(
                    e, vx[:, 2 * h * VD : (2 * h + 2) * VD], preferred_element_type=jnp.float32
                )
                maps.append(o[:, :VD] / o[:, VD:])
            mixed = maps[0] - lam_ref[z * heads + h] * maps[1]
            norm = lax.rsqrt(jnp.mean(mixed * mixed, axis=-1, keepdims=True) + 1e-06)
            osend[i, :, cols] = (mixed * norm * gain_ref[...]).astype(jnp.bfloat16)

        @pl.when(zq != z)
        def _():
            o_copy(i).start()

        if nz > 1:
            @pl.when(i == nz * per // 2)
            def _():
                w_take(1)

        return carry

    lax.fori_loop(0, nz * per, block, 0)
    if nz > 2:
        for copy in w_copies(1):
            copy.start()
    elif nz == 2:
        pass
    for j in range(per):
        att[j * block_rows : (j + 1) * block_rows, pl.ds(pl.multiple_of(z * own, 128), own)] = osend[(nz - 1) * per + j]
    if nz > 1:
        w_turn(1)
    for d in range(2, nz - 1):
        w_take(d)
    for d in range(1, nz):
        zp = lax.rem(z + d, nz)
        for j in range(per):
            to = att.at[pl.ds(j * block_rows, block_rows), pl.ds(pl.multiple_of(zp * own, 128), own)]
            remote(osend.at[j], to, o_s.at[j], o_r.at[zp, j], za=zp).wait_recv()

    def split(part):
        if nc == 1:
            return part, None
        low, high = part[:rows], part[rows:]
        return jnp.where(c == 0, low, high), jnp.where(c == 0, high, low)

    def oc_copy(e):
        return remote(oc_send.at[e], oc_recv.at[e], oc_s.at[e], oc_r.at[e], cb=other)

    def ox_copy(e):
        return remote(ox_send.at[e], ox_recv.at[e], ox_s.at[e], ox_r.at[e], xb=lax.rem(x + e, nx))

    ring = list(range(1, nx)) + [0]
    for e in ring:
        xp = lax.rem(x + e, nx)
        part = jnp.dot(
            att[pl.ds(pl.multiple_of(xp * pair, 8), pair)], ow[...], preferred_element_type=jnp.float32
        )
        keep, send = split(part)
        om[e] = keep
        if nc > 1:
            oc_send[e] = send.astype(jnp.bfloat16)
            oc_copy(e).start()
    for e in ring:
        total = om[e]
        if nc > 1:
            oc_copy(e).wait_recv()
            total = total + oc_recv[e].astype(jnp.float32)
        if e:
            ox_send[e] = total.astype(jnp.bfloat16)
            ox_copy(e).start()
    for d in range(2, nz - 1):
        w_turn(d)
    after = res[...].astype(jnp.float32) + total
    for e in range(1, nx):
        ox_copy(e).wait_recv()
        after = after + ox_recv[e].astype(jnp.float32)
    om[0] = after
    row_scale = lax.rsqrt(jnp.mean(after * after, axis=-1, keepdims=True) + 1e-06)

    def slot(zp, cc):
        return got.at[zp, pl.ds(pl.multiple_of(cc * rows, 8), rows)]

    def ag_z(zp, to):
        return remote(slot(zp, c), slot(zp, c), az_s.at[zp, jnp.where(to > z, 1, 0)], az_r.at[zp], za=to)

    def ag_c(zp):
        return remote(slot(zp, c), slot(zp, c), ac_s.at[zp], ac_r.at[zp], cb=other)

    def rs_c(zp):
        return remote(c_send.at[zp], c_recv.at[zp], rc_s.at[zp], rc_r.at[zp], cb=other)

    def rs_z(zp):
        return remote(z_send.at[zp], z_recv.at[z], rz_s.at[zp], rz_r.at[z], za=zp)

    got[z, pl.ds(pl.multiple_of(c * rows, 8), rows)] = (after * row_scale * ngain_ref[...]).astype(jnp.bfloat16)

    def onward(zp, act):
        to = jnp.where(zp < z, z + 1, z - 1)

        @pl.when(jnp.logical_and(to >= 0, to < nz))
        def _():
            act(ag_z(zp, to))

    def own_ways(act):
        @pl.when(z + 1 < nz)
        def _():
            act(ag_z(z, z + 1))

        @pl.when(z > 0)
        def _():
            act(ag_z(z, z - 1))

    own_ways(lambda copy: copy.start())
    if nc > 1:
        ag_c(z).start()

    def pass_on(k):
        zp = near_first(z, k, nz)
        ag_z(zp, jnp.where(zp < z, z - 1, z + 1)).wait_recv()
        onward(zp, lambda copy: copy.start())
        if nc > 1:
            ag_c(zp).start()

    contract = (((1,), (1,)), ((), ()))

    def compute(k):
        zp = near_first(z, k, nz)
        if nc > 1:
            remote(slot(zp, other), slot(zp, other), ac_s.at[zp], ac_r.at[zp], cb=other).wait_recv()
        tokens_in = got[zp]
        gate = lax.dot_general(tokens_in, w[0], contract, preferred_element_type=jnp.float32)
        up = lax.dot_general(tokens_in, w[1], contract, preferred_element_type=jnp.float32)
        hidden = (jax.nn.silu(gate) * up).astype(jnp.bfloat16)
        keep, send = split(jnp.dot(hidden, w[2], preferred_element_type=jnp.float32))
        mine[zp] = keep
        if nc > 1:
            c_send[zp] = send.astype(jnp.bfloat16)
            rs_c(zp).start()

    def finish(k):
        zp = near_first(z, k, nz)
        total = mine[zp]
        if nc > 1:
            rs_c(zp).wait_recv()
            total = total + c_recv[zp].astype(jnp.float32)
        if k:
            z_send[zp] = total.astype(jnp.bfloat16)
            rs_z(zp).start()
        return total

    if nz > 1:
        if nz > 2:
            w_take(nz - 1)
        pass_on(1)
        if nz > 2:
            w_turn(nz - 1)
    for k in range(2, nz - 1):
        pass_on(k)
    w_done()
    order = list(range(1, nz)) + [0]
    for i, k in enumerate(order):
        if k == nz - 1 and nz > 2:
            pass_on(k)
        compute(k)
        if i:
            finish(order[i - 1])
    total = finish(0)
    for k in range(1, nz):
        zp = near_first(z, k, nz)
        remote(z_send.at[zp], z_recv.at[zp], rz_s.at[zp], rz_r.at[zp], za=zp).wait_recv()
        total = total + z_recv[zp].astype(jnp.float32)
    out[...] = (om[0] + 0.5 * total).astype(jnp.bfloat16)

    for d in range(1, nz):
        for copy in qkv_copies(d) + w_copies(d):
            copy.wait_send()
    for d in range(nz):
        for f in range(1, ny):
            for copy in kv_pass(d, f):
                copy.wait_send()
            w_y(d, f).wait_send()
        for e in range(1, nx):
            w_x(d, e).wait_send()
            for f in range(1, ny):
                w_xy(d, e, f).wait_send()
                w_yx(d, f, e).wait_send()
    for i in range((nz - 1) * per):
        o_copy(i).wait_send()
    for e in range(nx):
        if nc > 1:
            oc_copy(e).wait_send()
        if e:
            ox_copy(e).wait_send()
    own_ways(lambda copy: copy.wait_send())
    for k in range(nz):
        zp = near_first(z, k, nz)
        if k:
            onward(zp, lambda copy: copy.wait_send())
            rs_z(zp).wait_send()
        if nc > 1:
            ag_c(zp).wait_send()
            rs_c(zp).wait_send()


def body(
    residual_in,
    queries,
    keys,
    values,
    mix_lambda,
    head_gain,
    out_weight,
    norm_gain,
    gate_weight,
    up_weight,
    down_weight,
):
    nz, ny, nx, nc = (lax.axis_size(name) for name in AXES)
    tok, width = queries.shape
    rows, model = residual_in.shape
    heads = mix_lambda.shape[0] // nz
    own = width // nz
    depth = down_weight.shape[1]
    hid = down_weight.shape[0] // nz
    aligned = depth % 128 == 0
    nsp = nz * ny
    block_rows = 2 * rows
    per = tok // block_rows
    vmem = pl.BlockSpec(memory_space=pltpu.VMEM)
    smem = pl.BlockSpec(memory_space=pltpu.SMEM)
    hbm = pl.BlockSpec(memory_space=pl.ANY)
    dma = pltpu.SemaphoreType.DMA
    bf16, f32 = jnp.bfloat16, jnp.float32
    parts = (8, 128) if aligned else (3, nx * hid, depth)
    return pl.pallas_call(
        functools.partial(layer_kernel, (nz, ny, nx, nc, heads, aligned)),
        out_shape=(
            jax.ShapeDtypeStruct((rows, model), bf16),
            jax.ShapeDtypeStruct(parts if aligned else (nsp, *parts), bf16),
        ),
        in_specs=[smem, vmem, vmem] + [hbm] * 8,
        out_specs=(vmem, hbm),
        scratch_shapes=[
            pltpu.VMEM((nz, tok, own), bf16),
            pltpu.VMEM((nsp * tok, own), bf16),
            pltpu.VMEM((nsp * tok, 2 * own), bf16),
            pltpu.VMEM((nz * per, block_rows, own), bf16),
            pltpu.VMEM((tok, width), bf16),
            pltpu.VMEM((width, model), bf16),
            pltpu.VMEM((rows, model), bf16),
            pltpu.VMEM((3, nx * hid, model), bf16),
            pltpu.VMEM(parts, bf16),
            pltpu.VMEM((nx, rows, model), f32),
            pltpu.VMEM((nx, rows, model), bf16),
            pltpu.VMEM((nx, rows, model), bf16),
            pltpu.VMEM((nx, rows, model), bf16),
            pltpu.VMEM((nx, rows, model), bf16),
            pltpu.VMEM((nz, nc * rows, model), bf16),
            pltpu.VMEM((nz, rows, model), f32),
            pltpu.VMEM((nz, rows, model), bf16),
            pltpu.VMEM((nz, rows, model), bf16),
            pltpu.VMEM((nz, rows, model), bf16),
            pltpu.VMEM((nz, rows, model), bf16),
            dma((heads + 4,)), dma,
            dma((heads + 2, nz)), dma((heads + 2, nz)),
            dma((heads + 1, nz, ny)), dma((heads + 1, nz, ny)),
            dma((3,)),
            dma((3, nz)), dma((3, nz)),
            dma((nz, nx)), dma((nz, nx)),
            dma((nz, ny)), dma((nz, ny)),
            dma((nz, nx, ny)), dma((nz, nx, ny)),
            dma((nz, ny, nx)), dma((nz, ny, nx)),
            dma((nz * per,)), dma((nz, per)),
            dma((nx,)), dma((nx,)),
            dma((nx,)), dma((nx,)),
            dma((nz, 2)), dma((nz,)),
            dma((nz,)), dma((nz,)),
            dma((nz,)), dma((nz,)),
            dma((nz,)), dma((nz,)),
        ],
        compiler_params=pltpu.CompilerParams(
            collective_id=1, has_side_effects=True, vmem_limit_bytes=62 * 1024 * 1024
        ),
    )(
        mix_lambda,
        head_gain.reshape(1, VD),
        norm_gain.reshape(1, model),
        residual_in,
        queries,
        keys,
        values,
        out_weight,
        gate_weight.T,
        up_weight.T,
        down_weight,
    )[0]


def solution(mesh):
    sp, tp = mesh.shape["sp"], mesh.shape["tp"]

    def run(*args):
        heads_local = args[4].shape[0] // tp
        za = math.gcd(heads_local, sp)
        nc = math.gcd(tp, 2)
        cut = Mesh(mesh.devices.reshape(za, sp // za, tp // nc, nc), AXES)
        s, t = ("za", "yb"), ("xb", "cb")
        return jax.shard_map(
            body,
            mesh=cut,
            in_specs=(
                P(AXES, None),
                P(s, t),
                P(s, t),
                P(s, t),
                P(t),
                P(),
                P(t, None),
                P(),
                P(s, t),
                P(s, t),
                P(t, s),
            ),
            out_specs=P(AXES, None),
            check_vma=False,
        )(*args)

    return run
```

time: 249 us -> 211 us (0.85)
  Pallas kernels: 218 us -> 204 us
  between operations: 13.6 us -> 0.01 us
  matrix products: 4.98 us -> 0 us
  local copies, waits for them, and re-layouts: 9.03 us -> 6.26 us
    pallas_call x2 -> x1, Pallas kernels: 218 us -> 204 us  [body(): pl.pallas_call(functools.partial(layer_kernel, (nz, ny, nx, nc, heads, al...]
    dot_general x1 -> x0, matrix products: 4.98 us -> none  [body(): jnp.dot(attended, out_full, preferred_element_type=jnp.float32)]
    unnamed x26 -> x3, local copies, waits for them, and re-layouts: 3.45 us -> 6.26 us
  transfers between devices with their start and end apart: 1 -> 0, of which waited for: 0 -> 0; matrix products, arithmetic and copies ran while one was open for 3% -> 0% of each run, Pallas kernels for 45% -> 0%
where the time goes in v1:
time: 211 us
  Pallas kernels  204 us (97%)
  local copies, waits for them, and re-layouts  6.26 us (3%)
    pallas_call x1, Pallas kernels, body(): pl.pallas_call(functools.partial(layer_kernel, (nz, ny, nx, nc, heads, al...  204 us
    unnamed x3, local copies, waits for them, and re-layouts  6.26 us

profile of v1, /device:TPU:0, one launch (start us, length us, event | category | flops | bytes accessed | tf_op | source)
XLA Modules:
  0.0 210.7 jit_solution(5386002792193792954)
XLA Ops:
  0.0 2.2 %copy.12 = bf16[256,1408]{0,1:T(8,128)(2,1)} copy(bf16[256,1408]{1,0:T(8,128)(2,1)} %param.19) | data formatting | bytes 1441792 | tf_op args[8]
  2.2 2.2 %copy.13 = bf16[256,1408]{0,1:T(8,128)(2,1)} copy(bf16[256,1408]{1,0:T(8,128)(2,1)} %param.20) | data formatting | bytes 1441792 | tf_op args[9]
  4.5 204.4 %shard_map.109 = (bf16[96,2048]{1,0:T(8,128)(2,1)}, bf16[8,128]{1,0:T(8,128)(2,1)}) custom-call(f32[4]{0:T(128)} %lam_ref.1, f32[1,128]{1,0:T(1,128)} %bitcast.7, f32[1,2048]{1,0:T(1,128)} %bitcast.6, bf16[96,2048]{1,0:T(8,128)(2,1)} %res_hbm.1, bf16[384,512]{1,0:T(8,128)(2,1)} %q_hbm.1, bf16[384,512]{1,0:T(8,128)(2,1)} %k_hbm.1, bf16[384,512]{1,0:T(8,128)(2,1)} %v_hbm.1, ...), custom_call_target="tpu_custom_call" | custom-call | tf_op jit(solution)/shard_map/pallas_call | solution.py:483
  208.9 1.8 copy.15

commit v2 on v1

--- a/solution.py
+++ b/solution.py
@@ -22,20 +22,20 @@
     )
 
 
-def near_first(z, k, nz):
-    m = jnp.minimum(z, nz - 1 - z)
-    near = z + ((k + 1) // 2 if k % 2 else -(k // 2))
-    far = jnp.where(z < nz - 1 - z, k, nz - 1 - k)
-    return jnp.where(k <= 2 * m, near, far)
+def across_first(z, k, nz):
+    half = max(nz // 2, 1)
+    if k < nz - half:
+        return jnp.where(z < half, half + k, half - 1 - k)
+    return z // half * half + lax.rem(z + 1 + k - (nz - half), half)
 
 
 def layer_kernel(n, lam_ref, gain_ref, ngain_ref, res_hbm, q_hbm, k_hbm, v_hbm, ow_hbm, gate_hbm, up_hbm, down_hbm,
                  out, wp,
                  qs, kk, vx, osend, att, ow, res, w, stage, om, oc_send, oc_recv, ox_send, ox_recv,
-                 got, mine, c_send, c_recv, z_send, z_recv,
+                 got, mine, c_send, c_recv, z_send, z_recv, t_recv,
                  in_s, st_s, qz_s, qz_r, ky_s, ky_r, wl_s, wz_s, wz_r, wx_s, wx_r, wy_s, wy_r,
                  wxy_s, wxy_r, wyx_s, wyx_r, o_s, o_r, oc_s, oc_r, ox_s, ox_r,
-                 az_s, az_r, ac_s, ac_r, rc_s, rc_r, rz_s, rz_r):
+                 az_s, az_r, ac_s, ac_r, rc_s, rc_r, rz_s, rz_r, rt_r):
     nz, ny, nx, nc, heads, aligned = n
     z, y, x, c = (lax.axis_index(name) for name in AXES)
     other = nc - 1 - c
@@ -137,9 +137,11 @@
         at = place(every, x, zp, yp, cut, hid - cut)
         return remote(at, at, wyx_s.at[d, f, e], wyx_r.at[zp, yp, x], xb=xp)
 
-    def w_spread(d):
+    def w_spread_x(d):
         for e in range(1, nx):
             w_x(d, e).start()
+
+    def w_spread_y(d):
         for f in range(1, ny):
             w_y(d, f).start()
 
@@ -147,7 +149,6 @@
         zp = lax.rem(z + d, nz)
         for m, a in enumerate(mats):
             remote(a.at[pl.ds(0, hid)], place(m, x, zp, y), wz_s.at[m, 0], wz_r.at[m, zp], za=zp).wait_recv()
-        w_spread(d)
 
     def w_turn(d):
         zp = lax.rem(z + d, nz)
@@ -195,33 +196,35 @@
             list(zip(kv_sources(z), kv_parts(z, y))) + [(q_source(z), qs.at[z]), (ow_hbm, ow), (res_hbm, res)]
         )
     ]
-    for copy in locals_in:
+    for copy in w_local() + locals_in:
         copy.start()
-    for copy in w_local():
-        copy.start()
-    for d in range(nz - 1, 1, -1):
-        for copy in w_copies(d):
-            copy.start()
     for h in range(heads):
         vx[:, (2 * h + 1) * VD : (2 * h + 2) * VD] = jnp.ones((vx.shape[0], VD), jnp.bfloat16)
     for copy in w_local():
         copy.wait()
-    w_spread(0)
+    w_spread_x(0)
+    w_spread_y(0)
     for copy in locals_in:
         copy.wait()
     for d in range(1, nz):
         zp = lax.rem(z + d, nz)
-        for copy in qkv_take(zp):
-            copy.wait_recv()
+        with jax.named_scope(f"qkv{d}"):
+            for copy in qkv_take(zp):
+                copy.wait_recv()
         for f in range(1, ny):
             for copy in kv_pass(d, f):
                 copy.start()
+    if nz > 1:
+        for copy in w_copies(nz - 1):
+            copy.start()
     for d in range(nz):
         zp = lax.rem(z + d, nz)
         for f in range(1, ny):
-            for copy in kv_take(zp, lax.rem(y + f, ny)):
-                copy.wait_recv()
-    w_turn(0)
+            with jax.named_scope(f"kv{d}"):
+                for copy in kv_take(zp, lax.rem(y + f, ny)):
+                    copy.wait_recv()
+    with jax.named_scope("turn0"):
+        w_turn(0)
 
     scale = LOG2E / math.sqrt(DH)
     block_rows = osend.shape[1]
@@ -261,29 +264,27 @@
             o_copy(i).start()
 
         if nz > 1:
-            @pl.when(i == nz * per // 2)
+            @pl.when(i == nz * per * 6 // 8)
             def _():
-                w_take(1)
+                with jax.named_scope("take1"):
+                    w_take(1)
+                    w_spread_x(1)
+                    w_spread_y(1)
 
         return carry
 
     lax.fori_loop(0, nz * per, block, 0)
+    for j in range(per):
+        att[j * block_rows : (j + 1) * block_rows, pl.ds(pl.multiple_of(z * own, 128), own)] = osend[(nz - 1) * per + j]
     if nz > 2:
         for copy in w_copies(1):
             copy.start()
-    elif nz == 2:
-        pass
-    for j in range(per):
-        att[j * block_rows : (j + 1) * block_rows, pl.ds(pl.multiple_of(z * own, 128), own)] = osend[(nz - 1) * per + j]
-    if nz > 1:
-        w_turn(1)
-    for d in range(2, nz - 1):
-        w_take(d)
     for d in range(1, nz):
         zp = lax.rem(z + d, nz)
-        for j in range(per):
-            to = att.at[pl.ds(j * block_rows, block_rows), pl.ds(pl.multiple_of(zp * own, 128), own)]
-            remote(osend.at[j], to, o_s.at[j], o_r.at[zp, j], za=zp).wait_recv()
+        with jax.named_scope(f"o_wait{d}"):
+            for j in range(per):
+                to = att.at[pl.ds(j * block_rows, block_rows), pl.ds(pl.multiple_of(zp * own, 128), own)]
+                remote(osend.at[j], to, o_s.at[j], o_r.at[zp, j], za=zp).wait_recv()
 
     def split(part):
         if nc == 1:
@@ -316,8 +317,17 @@
         if e:
             ox_send[e] = total.astype(jnp.bfloat16)
             ox_copy(e).start()
-    for d in range(2, nz - 1):
-        w_turn(d)
+    for d in range(nz - 2, 1, -1):
+        for copy in w_copies(d):
+            copy.start()
+    if nz > 2:
+        with jax.named_scope("take_third"):
+            w_take(nz - 1)
+            w_spread_x(nz - 1)
+            w_spread_y(nz - 1)
+    if nz > 1:
+        with jax.named_scope("turn1"):
+            w_turn(1)
     after = res[...].astype(jnp.float32) + total
     for e in range(1, nx):
         ox_copy(e).wait_recv()
@@ -328,8 +338,15 @@
     def slot(zp, cc):
         return got.at[zp, pl.ds(pl.multiple_of(cc * rows, 8), rows)]
 
-    def ag_z(zp, to):
-        return remote(slot(zp, c), slot(zp, c), az_s.at[zp, jnp.where(to > z, 1, 0)], az_r.at[zp], za=to)
+    half = max(nz // 2, 1)
+    outer = jnp.logical_or(z == 0, z == nz - 1)
+    gate_way = jnp.logical_or(z == half - 1, z == half)
+
+    def ag_z(zp, j, to):
+        return remote(slot(zp, c), slot(zp, c), az_s.at[zp, j], az_r.at[zp], za=to)
+
+    def near(j):
+        return z // half * half + lax.rem(z + j, half)
 
     def ag_c(zp):
         return remote(slot(zp, c), slot(zp, c), ac_s.at[zp], ac_r.at[zp], cb=other)
@@ -337,42 +354,78 @@
     def rs_c(zp):
         return remote(c_send.at[zp], c_recv.at[zp], rc_s.at[zp], rc_r.at[zp], cb=other)
 
+    inward = jnp.where(z < half, z + 1, z - 1)
+
+    def same(zp):
+        return z // half == zp // half
+
+    joined = (nz - half) // 2
+
+    def apart(zp):
+        return jnp.where(zp < half, half - 1 - zp, zp - half) >= joined
+
+    def at_once(zp):
+        return jnp.logical_or(same(zp), jnp.logical_or(outer, apart(zp)))
+
+    def straight(zp):
+        return jnp.logical_or(same(zp), jnp.logical_or(gate_way, apart(zp)))
+
     def rs_z(zp):
         return remote(z_send.at[zp], z_recv.at[z], rz_s.at[zp], rz_r.at[z], za=zp)
 
+    def rs_in(zp):
+        return remote(z_send.at[zp], t_recv.at[zp], rz_s.at[zp], rt_r.at[zp], za=inward)
+
+    def rs_act(zp, act):
+        @pl.when(straight(zp))
+        def _():
+            act(rs_z(zp))
+
+        if nz > 2:
+            @pl.when(jnp.logical_not(straight(zp)))
+            def _():
+                act(rs_in(zp))
+
     got[z, pl.ds(pl.multiple_of(c * rows, 8), rows)] = (after * row_scale * ngain_ref[...]).astype(jnp.bfloat16)
 
     def onward(zp, act):
-        to = jnp.where(zp < z, z + 1, z - 1)
-
-        @pl.when(jnp.logical_and(to >= 0, to < nz))
-        def _():
-            act(ag_z(zp, to))
+        if half > 1:
+            @pl.when(gate_way)
+            def _():
+                for j in range(1, half):
+                    act(ag_z(zp, j, near(j)))
 
     def own_ways(act):
-        @pl.when(z + 1 < nz)
-        def _():
-            act(ag_z(z, z + 1))
-
-        @pl.when(z > 0)
-        def _():
-            act(ag_z(z, z - 1))
-
-    own_ways(lambda copy: copy.start())
+        if nz > 1:
+            act(ag_z(z, 0, jnp.where(z < half, half, half - 1)))
+        for j in range(1, half):
+            act(ag_z(z, j, near(j)))
+
+    def own_near():
+        for j in range(1, half):
+            ag_z(z, j, near(j)).start()
+
+    if half > 1:
+        pl.when(outer)(own_near)
+    if nz > 1:
+        ag_z(z, 0, jnp.where(z < half, half, half - 1)).start()
+    if half > 1:
+        pl.when(jnp.logical_not(outer))(own_near)
     if nc > 1:
         ag_c(z).start()
 
     def pass_on(k):
-        zp = near_first(z, k, nz)
-        ag_z(zp, jnp.where(zp < z, z - 1, z + 1)).wait_recv()
-        onward(zp, lambda copy: copy.start())
+        zp = across_first(z, k, nz)
+        ag_z(zp, 0, zp).wait_recv()
+        if k < nz - half:
+            onward(zp, lambda copy: copy.start())
         if nc > 1:
             ag_c(zp).start()
 
     contract = (((1,), (1,)), ((), ()))
 
     def compute(k):
-        zp = near_first(z, k, nz)
+        zp = across_first(z, k, nz)
         if nc > 1:
             remote(slot(zp, other), slot(zp, other), ac_s.at[zp], ac_r.at[zp], cb=other).wait_recv()
         tokens_in = got[zp]
@@ -386,37 +439,78 @@
             rs_c(zp).start()
 
     def finish(k):
-        zp = near_first(z, k, nz)
+        zp = across_first(z, k, nz)
         total = mine[zp]
         if nc > 1:
             rs_c(zp).wait_recv()
             total = total + c_recv[zp].astype(jnp.float32)
-        if k:
-            z_send[zp] = total.astype(jnp.bfloat16)
-            rs_z(zp).start()
+        mine[zp] = total
+        if k < nz - 1:
+            @pl.when(at_once(zp))
+            def _():
+                z_send[zp] = total.astype(jnp.bfloat16)
+                rs_act(zp, lambda copy: copy.start())
         return total
 
-    if nz > 1:
-        if nz > 2:
-            w_take(nz - 1)
-        pass_on(1)
-        if nz > 2:
+    def gather_in(k):
+        zp = across_first(z, k, nz)
+
+        @pl.when(jnp.logical_not(outer))
+        def _():
+            rs_in(zp).wait_recv()
+            z_send[zp] = (mine[zp] + t_recv[zp].astype(jnp.float32)).astype(jnp.bfloat16)
+            rs_act(zp, lambda copy: copy.start())
+
+    if nz > 2:
+        with jax.named_scope("turn_third"):
             w_turn(nz - 1)
-    for k in range(2, nz - 1):
-        pass_on(k)
-    w_done()
-    order = list(range(1, nz)) + [0]
+    for d in range(2, nz - 1):
+        with jax.named_scope(f"take{d}"):
+            w_take(d)
+            w_spread_x(d)
+            w_spread_y(d)
+    def pass_across():
+        for k in range(nz - half):
+            with jax.named_scope(f"pass{k}"):
+                pass_on(k)
+
+    if half > 1:
+        pl.when(gate_way)(pass_across)
+    for d in range(2, nz - 1):
+        with jax.named_scope(f"turn{d}"):
+            w_turn(d)
+    for k in range(nz - half, nz - 1):
+        with jax.named_scope(f"pass{k}"):
+            pass_on(k)
+    with jax.named_scope("w_done"):
+        w_done()
+    order = list(range(max(nz - half - 1, 0))) + list(range(nz - half, nz - 1)) + list(range(max(nz - half - 1, 0), nz - half)) + [nz - 1]
     for i, k in enumerate(order):
-        if k == nz - 1 and nz > 2:
-            pass_on(k)
-        compute(k)
+        if k < nz - half:
+            late = functools.partial(pass_on, k)
+            with jax.named_scope(f"late_pass{k}"):
+                if half > 1:
+                    pl.when(jnp.logical_not(gate_way))(late)
+                else:
+                    late()
+        with jax.named_scope(f"compute{k}"):
+            compute(k)
         if i:
-            finish(order[i - 1])
-    total = finish(0)
-    for k in range(1, nz):
-        zp = near_first(z, k, nz)
-        remote(z_send.at[zp], z_recv.at[zp], rz_s.at[zp], rz_r.at[zp], za=zp).wait_recv()
-        total = total + z_recv[zp].astype(jnp.float32)
+            with jax.named_scope(f"finish{order[i - 1]}"):
+                finish(order[i - 1])
+    finish(order[-1])
+    if nz > 2:
+        for k in range(joined):
+            with jax.named_scope(f"gather_in{k}"):
+                gather_in(k)
+    for k in range(nz - 2, -1, -1):
+        zp = across_first(z, k, nz)
+        with jax.named_scope(f"rz{k}"):
+            @pl.when(jnp.logical_or(jnp.logical_or(same(zp), apart(z)), jnp.logical_or(zp == half - 1, zp == half)))
+            def _():
+                remote(z_send.at[zp], z_recv.at[zp], rz_s.at[zp], rz_r.at[zp], za=zp).wait_recv()
+                mine[z] = mine[z] + z_recv[zp].astype(jnp.float32)
+    total = mine[z]
     out[...] = (om[0] + 0.5 * total).astype(jnp.bfloat16)
 
     for d in range(1, nz):
@@ -441,10 +535,11 @@
             ox_copy(e).wait_send()
     own_ways(lambda copy: copy.wait_send())
     for k in range(nz):
-        zp = near_first(z, k, nz)
-        if k:
+        zp = across_first(z, k, nz)
+        if k < nz - half:
             onward(zp, lambda copy: copy.wait_send())
-            rs_z(zp).wait_send()
+        if k < nz - 1:
+            rs_act(zp, lambda copy: copy.wait_send())
         if nc > 1:
             ag_c(zp).wait_send()
             rs_c(zp).wait_send()
@@ -509,6 +604,7 @@
             pltpu.VMEM((nz, rows, model), bf16),
             pltpu.VMEM((nz, rows, model), bf16),
             pltpu.VMEM((nz, rows, model), bf16),
+            pltpu.VMEM((nz, rows, model), bf16),
             dma((heads + 4,)), dma,
             dma((heads + 2, nz)), dma((heads + 2, nz)),
             dma((heads + 1, nz, ny)), dma((heads + 1, nz, ny)),
@@ -521,10 +617,10 @@
             dma((nz * per,)), dma((nz, per)),
             dma((nx,)), dma((nx,)),
             dma((nx,)), dma((nx,)),
-            dma((nz, 2)), dma((nz,)),
+            dma((nz, max(nz // 2, 1))), dma((nz,)),
             dma((nz,)), dma((nz,)),
             dma((nz,)), dma((nz,)),
-            dma((nz,)), dma((nz,)),
+            dma((nz,)), dma((nz,)), dma((nz,)),
         ],
         compiler_params=pltpu.CompilerParams(
             collective_id=1, has_side_effects=True, vmem_limit_bytes=62 * 1024 * 1024

time: 211 us -> 165 us (0.78)
  Pallas kernels: 204 us -> 158 us
    pallas_call x1, Pallas kernels: 204 us -> 158 us  [body(): pl.pallas_call(functools.partial(layer_kernel, (nz, ny, nx, nc, heads, al...]
where the time goes in v2:
time: 165 us; the launch traced here: 164 us
  Pallas kernels  158 us (96%)
  local copies, waits for them, and re-layouts  6.26 us (4%)
    pallas_call x1, Pallas kernels, body(): pl.pallas_call(functools.partial(layer_kernel, (nz, ny, nx, nc, heads, al...  158 us
    unnamed x3, local copies, waits for them, and re-layouts  6.26 us

profile of v2, /device:TPU:0, one launch (start us, length us, event | category | flops | bytes accessed | tf_op | source)
XLA Modules:
  0.0 164.1 jit_solution(9104245459912262609)
XLA Ops:
  0.0 2.2 %copy.12 = bf16[256,1408]{0,1:T(8,128)(2,1)} copy(bf16[256,1408]{1,0:T(8,128)(2,1)} %param.19) | data formatting | bytes 1441792 | tf_op args[8]
  2.2 2.2 %copy.13 = bf16[256,1408]{0,1:T(8,128)(2,1)} copy(bf16[256,1408]{1,0:T(8,128)(2,1)} %param.20) | data formatting | bytes 1441792 | tf_op args[9]
  4.5 157.8 %shard_map.109 = (bf16[96,2048]{1,0:T(8,128)(2,1)}, bf16[8,128]{1,0:T(8,128)(2,1)}) custom-call(f32[4]{0:T(128)} %lam_ref.1, f32[1,128]{1,0:T(1,128)} %bitcast.7, f32[1,2048]{1,0:T(1,128)} %bitcast.6, bf16[96,2048]{1,0:T(8,128)(2,1)} %res_hbm.1, bf16[384,512]{1,0:T(8,128)(2,1)} %q_hbm.1, bf16[384,512]{1,0:T(8,128)(2,1)} %k_hbm.1, bf16[384,512]{1,0:T(8,128)(2,1)} %v_hbm.1, ...), custom_call_target="tpu_custom_call" | custom-call | tf_op jit(solution)/shard_map/pallas_call | solution.py:578
  162.3 1.8 %copy.15 = bf16[96,2048]{1,0:T(8,128)(2,1)} copy(bf16[96,2048]{1,0:T(8,128)(2,1)} %get-tuple-element.6) | data formatting | bytes 786432

commit v3 on v2

--- a/solution.py
+++ b/solution.py
@@ -29,11 +29,11 @@
     return z // half * half + lax.rem(z + 1 + k - (nz - half), half)
 
 
-def layer_kernel(n, lam_ref, gain_ref, ngain_ref, res_hbm, q_hbm, k_hbm, v_hbm, ow_hbm, gate_hbm, up_hbm, down_hbm,
+def layer_kernel(n, lam_ref, gain_ref, ngain_ref, res_hbm, q_hbm, k_hbm, v_hbm, ow_hbm, gate_in, up_in, down_hbm,
                  out, wp,
-                 qs, kk, vx, osend, att, ow, res, w, stage, om, oc_send, oc_recv, ox_send, ox_recv,
+                 qs, kk, vx, osend, att, ow, res, w, stage, raw, turned, om, oc_send, oc_recv, ox_send, ox_recv,
                  got, mine, c_send, c_recv, z_send, z_recv, t_recv,
-                 in_s, st_s, qz_s, qz_r, ky_s, ky_r, wl_s, wz_s, wz_r, wx_s, wx_r, wy_s, wy_r,
+                 in_s, st_s, raw_s, qz_s, qz_r, ky_s, ky_r, wl_s, wz_s, wz_r, wx_s, wx_r, wy_s, wy_r,
                  wxy_s, wxy_r, wyx_s, wyx_r, o_s, o_r, oc_s, oc_r, ox_s, ox_r,
                  az_s, az_r, ac_s, ac_r, rc_s, rc_r, rz_s, rz_r, rt_r):
     nz, ny, nx, nc, heads, aligned = n
@@ -42,7 +42,8 @@
     tok, own = qs.shape[1:]
     rows, model = res.shape
     pair = nc * rows
-    hid, depth = gate_hbm.shape[0] // nz, gate_hbm.shape[1]
+    hid, depth = down_hbm.shape[0] // nz, down_hbm.shape[1]
+    turn_here = gate_in.shape != down_hbm.shape
     cut = hid // 16 * 8
 
     barrier = pltpu.get_barrier_semaphore()
@@ -93,7 +94,7 @@
         to = kv_parts(zp, yp)
         return [remote(t, t, ky_s.at[i, 0, 0], ky_r.at[i, zp, yp], yb=yp) for i, t in enumerate(to)]
 
-    mats = (gate_hbm, up_hbm, down_hbm)
+    mats = (turned.at[0], turned.at[1], down_hbm) if turn_here else (gate_in, up_in, down_hbm)
 
     def place(m, xx, zz, yy, start=0, size=hid):
         at = zz * ny + yy
@@ -115,6 +116,7 @@
         return [
             pltpu.make_async_copy(a.at[pl.ds(pl.multiple_of(z * hid, 8), hid)], place(m, x, z, y), wl_s.at[m])
             for m, a in enumerate(mats)
+            if m == 2 or not turn_here
         ]
 
     def w_x(d, e):
@@ -196,10 +198,15 @@
             list(zip(kv_sources(z), kv_parts(z, y))) + [(q_source(z), qs.at[z]), (ow_hbm, ow), (res_hbm, res)]
         )
     ]
-    for copy in w_local() + locals_in:
+    raws = [pltpu.make_async_copy(a, raw.at[i], raw_s.at[i]) for i, a in enumerate((gate_in, up_in))] if turn_here else []
+    for copy in raws + w_local() + locals_in:
         copy.start()
     for h in range(heads):
         vx[:, (2 * h + 1) * VD : (2 * h + 2) * VD] = jnp.ones((vx.shape[0], VD), jnp.bfloat16)
+    for i, copy in enumerate(raws):
+        copy.wait()
+        turned[i] = raw[i].T
+        place(i, x, z, y)[...] = turned[i, pl.ds(pl.multiple_of(z * hid, 8), hid)]
     for copy in w_local():
         copy.wait()
     w_spread_x(0)
@@ -276,15 +283,19 @@
     lax.fori_loop(0, nz * per, block, 0)
     for j in range(per):
         att[j * block_rows : (j + 1) * block_rows, pl.ds(pl.multiple_of(z * own, 128), own)] = osend[(nz - 1) * per + j]
-    if nz > 2:
-        for copy in w_copies(1):
-            copy.start()
     for d in range(1, nz):
         zp = lax.rem(z + d, nz)
         with jax.named_scope(f"o_wait{d}"):
             for j in range(per):
                 to = att.at[pl.ds(j * block_rows, block_rows), pl.ds(pl.multiple_of(zp * own, 128), own)]
                 remote(osend.at[j], to, o_s.at[j], o_r.at[zp, j], za=zp).wait_recv()
+
+    if nz > 2:
+        for copy in w_copies(1):
+            copy.start()
+    for d in range(nz - 2, 1, -1):
+        for copy in w_copies(d):
+            copy.start()
 
     def split(part):
         if nc == 1:
@@ -317,9 +328,6 @@
         if e:
             ox_send[e] = total.astype(jnp.bfloat16)
             ox_copy(e).start()
-    for d in range(nz - 2, 1, -1):
-        for copy in w_copies(d):
-            copy.start()
     if nz > 2:
         with jax.named_scope("take_third"):
             w_take(nz - 1)
@@ -575,6 +583,10 @@
     dma = pltpu.SemaphoreType.DMA
     bf16, f32 = jnp.bfloat16, jnp.float32
     parts = (8, 128) if aligned else (3, nx * hid, depth)
+    turn_here = aligned and (nz * hid) % 128 == 0 and depth != nz * hid
+    gate, up = (gate_weight, up_weight) if turn_here else (gate_weight.T, up_weight.T)
+    raw = (2, *gate_weight.shape) if turn_here else (2, 8, 128)
+    turned = (2, *down_weight.shape) if turn_here else (2, 8, 128)
     return pl.pallas_call(
         functools.partial(layer_kernel, (nz, ny, nx, nc, heads, aligned)),
         out_shape=(
@@ -593,6 +605,8 @@
             pltpu.VMEM((rows, model), bf16),
             pltpu.VMEM((3, nx * hid, model), bf16),
             pltpu.VMEM(parts, bf16),
+            pltpu.VMEM(raw, bf16),
+            pltpu.VMEM(turned, bf16),
             pltpu.VMEM((nx, rows, model), f32),
             pltpu.VMEM((nx, rows, model), bf16),
             pltpu.VMEM((nx, rows, model), bf16),
@@ -605,7 +619,7 @@
             pltpu.VMEM((nz, rows, model), bf16),
             pltpu.VMEM((nz, rows, model), bf16),
             pltpu.VMEM((nz, rows, model), bf16),
-            dma((heads + 4,)), dma,
+            dma((heads + 4,)), dma, dma((2,)),
             dma((heads + 2, nz)), dma((heads + 2, nz)),
             dma((heads + 1, nz, ny)), dma((heads + 1, nz, ny)),
             dma((3,)),
@@ -634,8 +648,8 @@
         keys,
         values,
         out_weight,
-        gate_weight.T,
-        up_weight.T,
+        gate,
+        up,
         down_weight,
     )[0]
 

time: 165 us -> 159 us (0.964)
  local copies, waits for them, and re-layouts: 6.26 us -> 1.77 us
    unnamed x3 -> x1, local copies, waits for them, and re-layouts: 6.26 us -> 1.77 us
where the time goes in v3:
time: 159 us; the launch traced here: 158 us
  Pallas kernels  157 us (99%)
  local copies, waits for them, and re-layouts  1.77 us (1%)
    pallas_call x1, Pallas kernels, body(): pl.pallas_call(functools.partial(layer_kernel, (nz, ny, nx, nc, heads, al...  157 us

profile of v3, /device:TPU:0, one launch (start us, length us, event | category | flops | bytes accessed | tf_op | source)
XLA Modules:
  0.0 158.4 jit_solution(6786440156031484877)
XLA Ops:
  0.0 156.6 %shard_map.109 = (bf16[96,2048]{1,0:T(8,128)(2,1)}, bf16[8,128]{1,0:T(8,128)(2,1)}) custom-call(f32[4]{0:T(128)} %lam_ref.1, f32[1,128]{1,0:T(1,128)} %bitcast.3, f32[1,2048]{1,0:T(1,128)} %bitcast.2, bf16[96,2048]{1,0:T(8,128)(2,1)} %res_hbm.1, bf16[384,512]{1,0:T(8,128)(2,1)} %q_hbm.1, bf16[384,512]{1,0:T(8,128)(2,1)} %k_hbm.1, bf16[384,512]{1,0:T(8,128)(2,1)} %v_hbm.1, ...), custom_call_target="tpu_custom_call" | custom-call | tf_op jit(solution)/shard_map/pallas_call | solution.py:590
  156.6 1.8 %copy.13 = bf16[96,2048]{1,0:T(8,128)(2,1)} copy(bf16[96,2048]{1,0:T(8,128)(2,1)} %get-tuple-element.6) | data formatting | bytes 786432
